TPU v7x, 32 devices: a whole 2x2x4 slice. The times are simulated.
32 devices in a mesh: fs: 4 (over z), rep: 4 (over y, x), tp: 2 (over core).
Axes of the slice: x: 2, y: 2, z: 4, core: 2. Of those that a mesh axis runs over, the one named last changes fastest.
Arguments:
- saved_input: bfloat16 [16384, 2048], P(('fs', 'rep')), may hold values from -6 to 6
- value_cotangent: bfloat16 [16384, 4096], P(('fs', 'rep'), 'tp'), may hold values from -0.0061950684 to 0.0061950684
- factor: bfloat16 [2048, 128], P('fs'), may hold values from -1.5 to 1.5
- weight: float32 [2048, 4096], P('fs', 'tp'), may hold values from -1.2 to 1.2
- first_moment: float32 [128, 4096], P('fs', 'tp'), may hold values from -1.8 to 1.8
- second_moment: float32 [128, 4096], P('fs', 'tp'), may hold values from 0.1 to 1
Outputs:
- low_grad: float32 [128, 4096], P('fs', 'tp')
- new_first: float32 [128, 4096], P('fs', 'tp')
- new_second: float32 [128, 4096], P('fs', 'tp')
- direction: float32 [2048, 4096], P('fs', 'tp')
- new_weight: float32 [2048, 4096], P('fs', 'tp')
- new_copy: bfloat16 [2048, 4096], P('fs', 'tp')
All inputs are finite; a program needn't handle non-finite values.
Results may differ from a plain program's by a relative error of at most 0.006.
Values may be sent and summed in bfloat16 or wider, within the bound.
A program may use at most 64 MiB of HBM per device.

v0:
```python
import jax
import jax.numpy as jnp
from jax import lax
from jax.sharding import PartitionSpec as P

D = 2048
E = 4096
first_decay = 0.9
second_decay = 0.9
learn_rate = 0.05
epsilon = 1e-08


def on_device(saved_input, value_cotangent, factor, weight, first_moment, second_moment):
    factor_wide = factor.astype(jnp.float32)
    factor_whole = lax.all_gather(factor, "fs", axis=0, tiled=True)
    projected = jnp.dot(saved_input, factor_whole, preferred_element_type=jnp.float32)
    upper = projected.astype(jnp.bfloat16)
    lower = (projected - upper.astype(jnp.float32)).astype(jnp.bfloat16)
    dims = (((0,), (0,)), ((), ()))
    high_part = lax.dot_general(upper, value_cotangent, dims, preferred_element_type=jnp.float32)
    low_part = lax.dot_general(lower, value_cotangent, dims, preferred_element_type=jnp.float32)
    low_grad = lax.psum_scatter(high_part + low_part, "fs", scatter_dimension=0, tiled=True)
    low_grad = lax.psum(low_grad, "rep")
    new_first = first_decay * first_moment + (1.0 - first_decay) * low_grad
    new_second = second_decay * second_moment + (1.0 - second_decay) * low_grad * low_grad
    ratio = new_first / (jnp.sqrt(new_second) + epsilon)
    ratio_whole = lax.all_gather(ratio, "fs", axis=0, tiled=True)
    raw = jnp.dot(factor_wide, ratio_whole, precision=lax.Precision.HIGHEST)
    total = lax.psum(jnp.sum(raw * raw), ("fs", "tp"))
    spread = jnp.sqrt(total / (D * E))
    direction = raw / (spread + 1.0)
    new_weight = weight - learn_rate * direction
    return (low_grad, new_first, new_second, direction, new_weight, new_weight.astype(jnp.bfloat16))


def solution(mesh):
    placed = (
        P(("fs", "rep"), None),
        P(("fs", "rep"), "tp"),
        P("fs", None),
        P("fs", "tp"),
        P("fs", "tp"),
        P("fs", "tp"),
    )
    return jax.shard_map(
        on_device,
        mesh=mesh,
        in_specs=placed,
        out_specs=(
            P("fs", "tp"),
            P("fs", "tp"),
            P("fs", "tp"),
            P("fs", "tp"),
            P("fs", "tp"),
            P("fs", "tp"),
        ),
        check_vma=False,
    )
```

profile of v0, /device:TPU:0, one launch (start us, length us, event | category | flops | bytes accessed | tf_op | source)
XLA Modules:
  0.0 185.3 jit_solution(11213346444921834174)
XLA Ops:
  7.2 0.0 reduce-scatter.2.cloned.1.call-start
  7.2 17.7 %all_gather.6 = bf16[2048,128]{1,0:T(8,128)(2,1)S(1)} all-gather(bf16[512,128]{1,0:T(8,128)(2,1)} %param.8), channel_id=1, replica_groups=mesh['fs'=4,'rep'=4,'tp'=2] {'fs'}, dimensions={0}, use_global_device_ids=true | all-gather | bytes 655360 | tf_op jit(solution)/shard_map/all_gather | solution.py:16
  24.9 3.4 %fusion.6 = f32[1024,128]{1,0:T(8,128)S(1)} fusion(bf16[1024,2048]{1,0:T(8,128)(2,1)} %param.6, bf16[2048,128]{1,0:T(8,128)(2,1)S(1)} %all_gather.6), kind=kOutput, calls=%fused_computation.13 | convolution fusion | flops 536870912 | bytes 5242880 | tf_op jit(solution)/shard_map/dot_general | solution.py:17
  28.4 0.7 fusion.2
  29.1 0.0 copy-start.3
  29.2 1.7 convolution_add_fusion
  30.9 0.0 reduce-scatter.2.cloned.1.call-update
  30.9 0.0 all-reduce.2.cloned.1.call-start
  31.0 29.2 %reduce-scatter.2.cloned.1.call-done = f32[32,2048]{1,0:T(8,128)} async-done(((f32[128,2048]{1,0:T(8,128)}), f32[32,2048]{1,0:T(8,128)}) %reduce-scatter.2.cloned.1.call-update) | async-done | bytes 262160 | tf_op jit(solution)/shard_map/reduce_scatter | solution.py:23
  60.1 0.0 all-reduce.2.cloned.1.call-update
  60.1 0.0 all-gather.2.cloned.1.call-start
  60.2 44.5 %all-reduce.2.cloned.1.call-done = f32[32,2048]{1,0:T(8,128)} async-done(((f32[32,2048]{1,0:T(8,128)}), f32[32,2048]{1,0:T(8,128)}) %all-reduce.2.cloned.1.call-update) | async-done | bytes 262160 | tf_op jit(solution)/shard_map/psum | solution.py:24
  104.6 1.9 %add_divide_fusion = (f32[32,2048]{1,0:T(8,128)}, f32[32,2048]{1,0:T(8,128)}, f32[32,2048]{1,0:T(8,128)}) fusion(f32[32,2048]{1,0:T(8,128)} %all-reduce.2.cloned.1.call-done, f32[32,2048]{1,0:T(8,128)S(1)} %copy-done.3, f32[32,2048]{1,0:T(8,128)S(1)} %copy-done.4), kind=kLoop, calls=%fused_computation.8 | loop fusion | flops 524288 | bytes 1572864 | tf_op jit(solution)/shard_map/div | solution.py:27
  106.5 0.0 all-gather.2.cloned.1.call-update
  106.6 0.0 copy-start.2
  106.6 5.4 %copy.12 = f32[512,2048]{0,1:T(8,128)} copy(f32[512,2048]{1,0:T(8,128)} %param.9) | data formatting | bytes 8388608 | tf_op args[3]
  112.0 22.8 %all-gather.2.cloned.1.call-done = f32[128,2048]{1,0:T(8,128)} async-done(((f32[32,2048]{1,0:T(8,128)}), f32[128,2048]{1,0:T(8,128)}) %all-gather.2.cloned.1.call-update) | async-done | bytes 1048592 | tf_op jit(solution)/shard_map/all_gather | solution.py:28
  134.8 6.0 %multiply_reduce_fusion = (f32[]{:T(128)}, f32[2048,512]{1,0:T(8,128)}) fusion(f32[128,2048]{1,0:T(8,128)} %all-gather.2.cloned.1.call-done, bf16[512,128]{1,0:T(8,128)(2,1)S(1)} %copy-done.2), kind=kOutput, calls=%fused_computation.2 | convolution fusion | flops 1612709888 | bytes 5373956 | tf_op jit(solution)/shard_map/dot_general | solution.py:29
  140.8 15.3 %psum.15 = f32[]{:T(128)} all-reduce(f32[]{:T(128)} %get-tuple-element.18), channel_id=1, replica_groups=mesh['fs'=4,'rep'=4,'tp'=2] {'fs','tp'}, use_global_device_ids=true, to_apply=%region_3.0 | all-reduce | flops 1 | bytes 8 | tf_op jit(solution)/shard_map/psum | solution.py:30
  156.7 8.3 %fusion.4 = (bf16[512,2048]{0,1:T(8,128)(2,1)S(1)}, f32[512,2048]{0,1:T(8,128)}, f32[512,2048]{0,1:T(8,128)}) fusion(f32[512,2048]{0,1:T(8,128)} %copy.12, f32[2048,512]{1,0:T(8,128)} %get-tuple-element.19, f32[]{:T(128)S(6)} %add.29), kind=kLoop, calls=%fused_computation.12 | loop fusion | flops 4194304 | bytes 18874372 | tf_op jit(solution)/shard_map/convert_element_type | solution.py:34
  165.0 2.4 %copy.15 = bf16[512,2048]{1,0:T(8,128)(2,1)} copy(bf16[512,2048]{0,1:T(8,128)(2,1)S(1)} %get-tuple-element.12) | data formatting | bytes 4194304
  167.4 5.3 %copy.14 = f32[512,2048]{1,0:T(8,128)} copy(f32[512,2048]{0,1:T(8,128)} %get-tuple-element.13) | data formatting | bytes 8388608
  172.7 5.4 %copy.13 = f32[512,2048]{1,0:T(8,128)} copy(f32[512,2048]{0,1:T(8,128)} %get-tuple-element.14) | data formatting | bytes 8388608
  178.1 0.7 copy.17
  (8 shorter events, 0.0 us)
Async XLA Ops:
  7.2 52.9 %reduce-scatter.2.cloned.1.call-start = ((), (), s32[]{:S(2)}) async-start(), calls=%async_computation.1 | async-start | bytes 1310720 | tf_op jit(solution)/shard_map/reduce_scatter | solution.py:23
  7.2 21.2 %copy-start = (bf16[1024,2048]{1,0:T(8,128)(2,1)S(1)}, bf16[1024,2048]{1,0:T(8,128)(2,1)}, u32[]{:S(2)}) copy-start(bf16[1024,2048]{1,0:T(8,128)(2,1)} %param.7) | copy-start | bytes 12582916
  29.1 75.5 %copy-start.3 = (f32[32,2048]{1,0:T(8,128)S(1)}, f32[32,2048]{1,0:T(8,128)}, u32[]{:S(2)}) copy-start(f32[32,2048]{1,0:T(8,128)} %param.11) | copy-start | bytes 786436
  29.1 75.5 %copy-start.4 = (f32[32,2048]{1,0:T(8,128)S(1)}, f32[32,2048]{1,0:T(8,128)}, u32[]{:S(2)}) copy-start(f32[32,2048]{1,0:T(8,128)} %param.10) | copy-start | bytes 786436
  30.9 73.7 %all-reduce.2.cloned.1.call-start = ((), (), s32[]{:S(2)}) async-start(), calls=%async_computation.2 | async-start | bytes 524288 | tf_op jit(solution)/shard_map/psum | solution.py:24
  60.1 74.7 %all-gather.2.cloned.1.call-start = ((), (), s32[]{:S(2)}) async-start(), calls=%async_computation.3 | async-start | bytes 1310720 | tf_op jit(solution)/shard_map/all_gather | solution.py:28
  106.6 28.2 %copy-start.2 = (bf16[512,128]{1,0:T(8,128)(2,1)S(1)}, bf16[512,128]{1,0:T(8,128)(2,1)}, u32[]{:S(2)}) copy-start(bf16[512,128]{1,0:T(8,128)(2,1)} %param.8) | copy-start | bytes 393220
  172.7 5.4 %copy-start.1 = (f32[32,2048]{1,0:T(8,128)S(1)}, f32[32,2048]{1,0:T(8,128)}, u32[]{:S(2)}) copy-start(f32[32,2048]{1,0:T(8,128)} %all-reduce.2.cloned.1.call-done) | copy-start | bytes 786436
Sparse Core Ops, SparseCore 0:
  31.0 29.0 reduce-scatter.1
  63.0 41.5 all-reduce.1
  106.8 27.9 all-gather.1
where the time goes:
time: 186 us; the launch traced here: 185 us
  waiting for transfers between devices  96.5 us (52%)
  blocking collectives  33 us (18%)
  local copies, waits for them, and re-layouts  19.2 us (10%)
  between operations  14.5 us (8%)
  matrix products  11.9 us (6%)
  other arithmetic  10.2 us (5%)
    psum x1, waiting for transfers between devices, on_device(): low_grad = lax.psum(low_grad, 'rep')  44.5 us
    reduce_scatter x1, waiting for transfers between devices, on_device(): lax.psum_scatter(high_part + low_part, 'fs', scatter_dimension=0, tiled=T...  29.2 us
    all_gather x1, waiting for transfers between devices, on_device(): ratio_whole = lax.all_gather(ratio, 'fs', axis=0, tiled=True)  22.8 us
    unnamed x15, local copies, waits for them, and re-layouts  19.2 us
    all_gather x1, blocking collectives, on_device(): factor_whole = lax.all_gather(factor, 'fs', axis=0, tiled=True)  17.7 us
    psum x1, blocking collectives, on_device(): total = lax.psum(jnp.sum(raw * raw), ('fs', 'tp'))  15.3 us
    convert_element_type x1, other arithmetic, on_device(): new_weight.astype(jnp.bfloat16)  8.28 us
    dot_general x1, matrix products, on_device(): raw = jnp.dot(factor_wide, ratio_whole, precision=lax.Precision.HIGHEST)  5.95 us
  transfers between devices with their start and end apart: 3, of which 3 were waited for; matrix products, arithmetic and copies ran while one was open for 3% of the time, Pallas kernels for 0%

commit v1 on v0

--- a/solution.py
+++ b/solution.py
@@ -11,6 +11,10 @@
 epsilon = 1e-08
 
 
+def edit_stacks_all_now(panel):
+    return jnp.sum(lax.all_gather(panel, "rep"), axis=0)
+
+
 def on_device(saved_input, value_cotangent, factor, weight, first_moment, second_moment):
     factor_wide = factor.astype(jnp.float32)
     factor_whole = lax.all_gather(factor, "fs", axis=0, tiled=True)
@@ -21,7 +25,7 @@
     high_part = lax.dot_general(upper, value_cotangent, dims, preferred_element_type=jnp.float32)
     low_part = lax.dot_general(lower, value_cotangent, dims, preferred_element_type=jnp.float32)
     low_grad = lax.psum_scatter(high_part + low_part, "fs", scatter_dimension=0, tiled=True)
-    low_grad = lax.psum(low_grad, "rep")
+    low_grad = edit_stacks_all_now(low_grad)
     new_first = first_decay * first_moment + (1.0 - first_decay) * low_grad
     new_second = second_decay * second_moment + (1.0 - second_decay) * low_grad * low_grad
     ratio = new_first / (jnp.sqrt(new_second) + epsilon)

time: 186 us -> 168 us (0.903)
  waiting for transfers between devices: 96.5 us -> 78.7 us
    psum x1 -> x0, waiting for transfers between devices: 44.5 us -> none  [on_device(): low_grad = lax.psum(low_grad, 'rep')]
    all_gather x0 -> x1, waiting for transfers between devices: none -> 26.8 us  [edit_stacks_all_now(): return jnp.sum(lax.all_gather(panel, 'rep'), axis=0)]
    unnamed x15 -> x14, local copies, waits for them, and re-layouts: 19.2 us -> 18.5 us
where the time goes in v1:
time: 168 us; the launch traced here: 167 us
  waiting for transfers between devices  78.7 us (47%)
  blocking collectives  33 us (20%)
  local copies, waits for them, and re-layouts  18.5 us (11%)
  between operations  14.5 us (9%)
  matrix products  11.8 us (7%)
  other arithmetic  10.6 us (6%)
    reduce_scatter x1, waiting for transfers between devices, on_device(): lax.psum_scatter(high_part + low_part, 'fs', scatter_dimension=0, tiled=T...  29.2 us
    all_gather x1, waiting for transfers between devices, edit_stacks_all_now(): return jnp.sum(lax.all_gather(panel, 'rep'), axis=0)  26.8 us
    all_gather x1, waiting for transfers between devices, on_device(): ratio_whole = lax.all_gather(ratio, 'fs', axis=0, tiled=True)  22.7 us
    unnamed x14, local copies, waits for them, and re-layouts  18.5 us
    all_gather x1, blocking collectives, on_device(): factor_whole = lax.all_gather(factor, 'fs', axis=0, tiled=True)  17.7 us
    psum x1, blocking collectives, on_device(): total = lax.psum(jnp.sum(raw * raw), ('fs', 'tp'))  15.3 us
    convert_element_type x1, other arithmetic, on_device(): new_weight.astype(jnp.bfloat16)  8.28 us
    dot_general x1, matrix products, on_device(): raw = jnp.dot(factor_wide, ratio_whole, precision=lax.Precision.HIGHEST)  5.95 us
  transfers between devices with their start and end apart: 3, of which 3 were waited for; matrix products, arithmetic and copies ran while one was open for 3% of the time, Pallas kernels for 0%

profile of v1, /device:TPU:0, one launch (start us, length us, event | category | flops | bytes accessed | tf_op | source)
XLA Modules:
  0.0 167.3 jit_solution(8018532814044504057)
XLA Ops:
  7.2 0.0 reduce-scatter.2.cloned.1.call-start
  7.2 17.7 %all_gather.12 = bf16[2048,128]{1,0:T(8,128)(2,1)S(1)} all-gather(bf16[512,128]{1,0:T(8,128)(2,1)} %param.8), channel_id=1, replica_groups=mesh['fs'=4,'rep'=4,'tp'=2] {'fs'}, dimensions={0}, use_global_device_ids=true | all-gather | bytes 655360 | tf_op jit(solution)/shard_map/all_gather | solution.py:20
  24.9 3.4 %fusion.6 = f32[1024,128]{1,0:T(8,128)S(1)} fusion(bf16[1024,2048]{1,0:T(8,128)(2,1)} %param.6, bf16[2048,128]{1,0:T(8,128)(2,1)S(1)} %all_gather.12), kind=kOutput, calls=%fused_computation.13 | convolution fusion | flops 536870912 | bytes 5242880 | tf_op jit(solution)/shard_map/dot_general | solution.py:21
  28.4 0.7 fusion.2
  29.1 0.0 copy-start.3
  29.2 1.7 %convolution_add_fusion = f32[128,2048]{1,0:T(8,128)} fusion(f32[128,2048]{1,0:T(8,128)S(1)} %fusion.2, bf16[1024,2048]{1,0:T(8,128)(2,1)S(1)} %copy-done, f32[1024,128]{1,0:T(8,128)S(1)} %fusion.6), kind=kOutput, calls=%fused_computation.3 | convolution fusion | flops 537657344 | bytes 6815744 | tf_op jit(solution)/shard_map/dot_general | solution.py:26
  30.9 0.0 reduce-scatter.2.cloned.1.call-update
  30.9 0.0 all-gather.6.cloned.1.call-start
  31.0 29.2 %reduce-scatter.2.cloned.1.call-done = f32[32,2048]{1,0:T(8,128)} async-done(((f32[128,2048]{1,0:T(8,128)}), f32[32,2048]{1,0:T(8,128)}) %reduce-scatter.2.cloned.1.call-update) | async-done | bytes 262160 | tf_op jit(solution)/shard_map/reduce_scatter | solution.py:27
  60.1 0.0 all-gather.6.cloned.1.call-update
  60.1 0.0 all-gather.4.cloned.1.call-start
  60.2 26.8 %all-gather.6.cloned.1.call-done = f32[128,2048]{1,0:T(8,128)} async-done(((f32[32,2048]{1,0:T(8,128)}), f32[128,2048]{1,0:T(8,128)}) %all-gather.6.cloned.1.call-update) | async-done | bytes 1048592 | tf_op jit(solution)/shard_map/all_gather | solution.py:15
  87.0 1.3 reduce_sum.18
  88.3 0.0 copy-start.1
  88.3 1.0 add_divide_fusion
  89.4 0.0 all-gather.4.cloned.1.call-update
  89.4 5.4 %copy.12 = f32[512,2048]{0,1:T(8,128)} copy(f32[512,2048]{1,0:T(8,128)} %param.9) | data formatting | bytes 8388608 | tf_op args[3]
  94.8 22.7 %all-gather.4.cloned.1.call-done = f32[128,2048]{1,0:T(8,128)} async-done(((f32[32,2048]{1,0:T(8,128)}), f32[128,2048]{1,0:T(8,128)}) %all-gather.4.cloned.1.call-update) | async-done | bytes 1048592 | tf_op jit(solution)/shard_map/all_gather | solution.py:32
  117.5 6.0 %multiply_reduce_fusion = (f32[]{:T(128)}, f32[2048,512]{1,0:T(8,128)}) fusion(f32[128,2048]{1,0:T(8,128)} %all-gather.4.cloned.1.call-done, bf16[512,128]{1,0:T(8,128)(2,1)S(1)} %copy-done.2), kind=kOutput, calls=%fused_computation.2 | convolution fusion | flops 1612709888 | bytes 5373956 | tf_op jit(solution)/shard_map/dot_general | solution.py:33
  123.5 15.3 %psum.7 = f32[]{:T(128)} all-reduce(f32[]{:T(128)} %get-tuple-element.18), channel_id=1, replica_groups=mesh['fs'=4,'rep'=4,'tp'=2] {'fs','tp'}, use_global_device_ids=true, to_apply=%region_3.0 | all-reduce | flops 1 | bytes 8 | tf_op jit(solution)/shard_map/psum | solution.py:34
  139.5 8.3 %fusion.4 = (bf16[512,2048]{0,1:T(8,128)(2,1)S(1)}, f32[512,2048]{0,1:T(8,128)}, f32[512,2048]{0,1:T(8,128)}) fusion(f32[512,2048]{0,1:T(8,128)} %copy.12, f32[2048,512]{1,0:T(8,128)} %get-tuple-element.19, f32[]{:T(128)S(6)} %add.27), kind=kLoop, calls=%fused_computation.12 | loop fusion | flops 4194304 | bytes 18874372 | tf_op jit(solution)/shard_map/convert_element_type | solution.py:38
  147.7 2.4 %copy.15 = bf16[512,2048]{1,0:T(8,128)(2,1)} copy(bf16[512,2048]{0,1:T(8,128)(2,1)S(1)} %get-tuple-element.12) | data formatting | bytes 4194304
  150.1 5.3 %copy.14 = f32[512,2048]{1,0:T(8,128)} copy(f32[512,2048]{0,1:T(8,128)} %get-tuple-element.13) | data formatting | bytes 8388608
  155.4 5.3 %copy.13 = f32[512,2048]{1,0:T(8,128)} copy(f32[512,2048]{0,1:T(8,128)} %get-tuple-element.14) | data formatting | bytes 8388608
  (8 shorter events, 0.0 us)
Async XLA Ops:
  7.2 52.9 %reduce-scatter.2.cloned.1.call-start = ((), (), s32[]{:S(2)}) async-start(), calls=%async_computation.1 | async-start | bytes 1310720 | tf_op jit(solution)/shard_map/reduce_scatter | solution.py:27
  7.2 21.2 %copy-start = (bf16[1024,2048]{1,0:T(8,128)(2,1)S(1)}, bf16[1024,2048]{1,0:T(8,128)(2,1)}, u32[]{:S(2)}) copy-start(bf16[1024,2048]{1,0:T(8,128)(2,1)} %param.7) | copy-start | bytes 12582916
  29.1 59.2 %copy-start.3 = (f32[32,2048]{1,0:T(8,128)S(1)}, f32[32,2048]{1,0:T(8,128)}, u32[]{:S(2)}) copy-start(f32[32,2048]{1,0:T(8,128)} %param.11) | copy-start | bytes 786436
  29.1 59.1 %copy-start.4 = (f32[32,2048]{1,0:T(8,128)S(1)}, f32[32,2048]{1,0:T(8,128)}, u32[]{:S(2)}) copy-start(f32[32,2048]{1,0:T(8,128)} %param.10) | copy-start | bytes 786436
  30.9 56.1 %all-gather.6.cloned.1.call-start = ((), (), s32[]{:S(2)}) async-start(), calls=%async_computation.3 | async-start | bytes 1310720 | tf_op jit(solution)/shard_map/all_gather | solution.py:15
  60.1 57.4 %all-gather.4.cloned.1.call-start = ((), (), s32[]{:S(2)}) async-start(), calls=%async_computation.2 | async-start | bytes 1310720 | tf_op jit(solution)/shard_map/all_gather | solution.py:32
  88.3 6.5 %copy-start.1 = (f32[32,2048]{1,0:T(8,128)}, f32[32,2048]{1,0:T(8,128)S(1)}, u32[]{:S(2)}) copy-start(f32[32,2048]{1,0:T(8,128)S(1)} %reduce_sum.18) | copy-start | bytes 786436
  89.4 28.1 %copy-start.2 = (bf16[512,128]{1,0:T(8,128)(2,1)S(1)}, bf16[512,128]{1,0:T(8,128)(2,1)}, u32[]{:S(2)}) copy-start(bf16[512,128]{1,0:T(8,128)(2,1)} %param.8) | copy-start | bytes 393220
Sparse Core Ops, SparseCore 0:
  31.0 29.0 reduce-scatter.1
  62.0 24.9 all-gather.5
  89.5 27.9 all-gather.3
